TPU v7x, 512 devices: a whole 4x4x16 slice. The times are simulated.
512 devices in a mesh: sp: 16 (over z), tp: 4 (over y), dp: 8 (over x, core).
Axes of the slice: x: 4, y: 4, z: 16, core: 2. Of those that a mesh axis runs over, the one named last changes fastest.
Arguments:
- latent: bfloat16 [32768, 2048], P(('dp', 'sp', 'tp')), parts along dimension 0, may hold values from -6 to 6
- context: bfloat16 [2048, 2048], P(('dp', 'sp')), parts along dimension 0, may hold values from -6 to 6
- cond: bfloat16 [16384], P(('dp', 'sp')), parts along dimension 0, may hold values from -6 to 6
- context_cond: bfloat16 [2048], P('sp'), may hold values from -6 to 6
- norm_gain: float32 [2048], replicated, may hold values from 0.1 to 1.9
- mod_shift: bfloat16 [2048, 2048], P('sp', 'tp'), may hold values from -0.125 to 0.125
- mod_scale: bfloat16 [2048, 2048], P('sp', 'tp'), may hold values from -0.125 to 0.125
- mod_gate: bfloat16 [2048, 2048], P('sp', 'tp'), may hold values from -0.125 to 0.125
- w_query: bfloat16 [2048, 1024], P(None, 'tp'), may hold values from -0.125 to 0.125
- w_key: bfloat16 [2048, 1024], P(None, 'tp'), may hold values from -0.125 to 0.125
- w_value: bfloat16 [2048, 1024], P(None, 'tp'), may hold values from -0.125 to 0.125
- query_gain: float32 [64], replicated, may hold values from 1.4 to 2.2
- key_gain: float32 [64], replicated, may hold values from 0.1 to 1.9
- mix_lambda: float32 [8], P('tp'), may hold values from 0.3 to 0.8
- context_lift: float32 [8], P('tp'), may hold values from 1.5 to 2.5
- value_gain: float32 [128], replicated, may hold values from 0.1 to 1.9
- w_out: bfloat16 [1024, 2048], P('tp'), may hold values from -0.1875 to 0.1875
Outputs:
- output: bfloat16 [32768, 2048], P(('dp', 'sp', 'tp')), parts along dimension 0
There are 8 independent parts, one for each index of `dp`. A program takes and returns all parts, laid end to end along the dimension named above; an argument that names none is the same for every part. Nothing has to cross between parts.
All inputs are finite; a program needn't handle non-finite values.
Results may differ from a plain program's by a relative error of at most 0.006.
Values may be sent and summed in bfloat16 or wider, within the bound.
A program may use at most 64 MiB of HBM per device.

v0:
```python
import jax
import jax.numpy as jnp
from jax import lax
from jax.sharding import PartitionSpec as P

GRID = 64
token_eps = 0.01
head_eps = 0.001
rope_base = 10000.0
head_factor = 0.8
key_block = 512


def copy_for_each(array, axis):
    copies = jnp.broadcast_to(array, (lax.axis_size(axis), *array.shape))
    return lax.all_to_all(copies, axis, split_axis=0, concat_axis=0, tiled=True)


def taken_together(array, axis):
    return copy_for_each(array, axis).sum(axis=0)


def in_order(tiles, dim):
    tiles = jnp.moveaxis(tiles, 0, dim)
    shape = tiles.shape
    return tiles.reshape(*shape[:dim], shape[dim] * shape[dim + 1], *shape[dim + 2 :])


def collect(array, axis, dim):
    tiles = copy_for_each(array, axis)
    return in_order(tiles, dim)


def sent_together(arrays, axis, dim, along):
    both = jnp.concatenate(arrays, axis=along)
    out, at, gathered = (lax.all_gather(both, axis, axis=dim, tiled=True), 0, [])
    for a in arrays:
        gathered.append(lax.slice_in_dim(out, at, at + a.shape[along], axis=along))
        at += a.shape[along]
    return tuple(gathered)


def cut_along(array, dim, devices):
    before, after = (array.shape[:dim], array.shape[dim + 1 :])
    return jnp.moveaxis(array.reshape(*before, devices, -1, *after), dim, 0)


def sum_at_owner(array, axis, dim):
    devices = lax.axis_size(axis)
    tiles = lax.all_to_all(cut_along(array, dim, devices), axis, 0, 0, tiled=True)
    return jnp.sum(tiles, axis=0)


def modulated_norm(row_block, gain_vector, shift_vector, scale_vector):
    values = row_block.astype(jnp.float32)
    inverse = lax.rsqrt(jnp.mean(values * values, axis=-1, keepdims=True) + token_eps)
    return (values * inverse * gain_vector * (1.0 + scale_vector) + shift_vector).astype(
        jnp.bfloat16
    )


def head_norm(values, gain_vector):
    inverse = lax.rsqrt(jnp.mean(values * values, axis=-1, keepdims=True) + token_eps)
    return values * inverse * gain_vector


def rotate(values, positions):
    quarter = values.shape[-1] // 4
    inverse = rope_base ** (-jnp.arange(quarter, dtype=jnp.float32) / quarter)
    grid_row = (positions // GRID).astype(jnp.float32)
    grid_col = (positions % GRID).astype(jnp.float32)
    angles = jnp.stack([grid_row[:, None] * inverse, grid_col[:, None] * inverse], axis=1)
    cosine_table = jnp.cos(angles)[:, None, None]
    sine_table = jnp.sin(angles)[:, None, None]
    halves = values.reshape(values.shape[:3] + (2, 2, quarter))
    front_half = halves[..., 0, :]
    back_half = halves[..., 1, :]
    turned = jnp.stack(
        [
            front_half * cosine_table - back_half * sine_table,
            back_half * cosine_table + front_half * sine_table,
        ],
        axis=-2,
    )
    return turned.reshape(values.shape)


def project_heads(row_block, weight, gain_vector, positions, factor):
    row_count = row_block.shape[0]
    head_width = gain_vector.shape[0]
    product = jnp.dot(row_block, weight, preferred_element_type=jnp.float32)
    shaped = head_norm(product.reshape(row_count, -1, 2, head_width), gain_vector)
    if positions is not None:
        shaped = rotate(shaped, positions)
    return (shaped * factor).astype(jnp.bfloat16).reshape(row_count, -1)


def accumulate(running, queries, key_slab, value_slab, lift_rows):
    numerator, totals = running
    head_count = lift_rows.shape[0]
    head_width = queries.shape[1] // (2 * head_count)
    shaped_query = queries.reshape(queries.shape[0], head_count, 2, head_width)
    shaped_keys = key_slab.reshape(key_slab.shape[0], head_count, 2, head_width)
    shaped_values = value_slab.reshape(value_slab.shape[0], head_count, -1)
    scores = jnp.einsum(
        "qhmd,phmd->mhqp", shaped_query, shaped_keys, preferred_element_type=jnp.float32
    )
    weights = jnp.exp(scores + lift_rows[None, :, None, :])
    totals = totals + jnp.sum(weights, axis=-1)
    numerator = numerator + jnp.einsum(
        "mhqp,phe->mhqe",
        weights.astype(jnp.bfloat16),
        shaped_values,
        preferred_element_type=jnp.float32,
    )
    return (numerator, totals)


def accumulate_blocks(running, queries, key_slab, value_slab, lift_rows):
    row_count = key_slab.shape[0]
    full_blocks = row_count // key_block
    covered = full_blocks * key_block
    head_count = lift_rows.shape[0]
    slabs = (
        key_slab[:covered].reshape(full_blocks, key_block, -1),
        value_slab[:covered].reshape(full_blocks, key_block, -1),
        jnp.transpose(
            lift_rows[:, :covered].reshape(head_count, full_blocks, key_block), (1, 0, 2)
        ),
    )

    def scan_step(inside, slab):
        return (accumulate(inside, queries, slab[0], slab[1], slab[2]), None)

    running = lax.scan(scan_step, running, slabs)[0]
    running = accumulate(
        running, queries, key_slab[covered:], value_slab[covered:], lift_rows[:, covered:]
    )
    return running


def on_device(
    latent,
    context,
    cond,
    context_cond,
    norm_gain,
    mod_shift,
    mod_scale,
    mod_gate,
    w_query,
    w_key,
    w_value,
    query_gain,
    key_gain,
    mix_lambda,
    context_lift,
    value_gain,
    w_out,
):
    cond_act = jax.nn.silu(cond.astype(jnp.float32)).astype(jnp.bfloat16)
    context_act = jax.nn.silu(context_cond.astype(jnp.float32)).astype(jnp.bfloat16)
    both_acts = jnp.stack([cond_act, context_act])
    shifts = jnp.dot(both_acts, mod_shift, preferred_element_type=jnp.float32)
    scales = jnp.dot(both_acts, mod_scale, preferred_element_type=jnp.float32)
    gates = jnp.dot(cond_act[None, :], mod_gate, preferred_element_type=jnp.float32)
    partial_mod = jnp.concatenate([shifts, scales, gates], axis=0)
    summed = taken_together(partial_mod, "sp")
    modulation = collect(summed, "tp", 1)
    normed = modulated_norm(latent, norm_gain, modulation[0], modulation[2])
    context_normed = modulated_norm(context, norm_gain, modulation[1], modulation[3])
    local_rows = latent.shape[0]
    offset = lax.axis_index("sp") * (local_rows * lax.axis_size("tp"))
    head_width = query_gain.shape[0]
    pieces = lax.all_gather(normed, "tp", axis=0, tiled=True)
    positions = offset + jnp.arange(pieces.shape[0], dtype=jnp.int32)
    query_part = project_heads(pieces, w_query, query_gain, positions, head_width ** (-0.5))
    key_part = project_heads(pieces, w_key, key_gain, positions, 1.0)
    value_part = jnp.dot(pieces, w_value, preferred_element_type=jnp.float32).astype(jnp.bfloat16)
    projected = jnp.concatenate([query_part, key_part, value_part], axis=1)
    qk_width = w_query.shape[1]
    queries = projected[:, :qk_width]
    latent_keys = projected[:, qk_width : 2 * qk_width]
    latent_values = projected[:, 2 * qk_width :]
    heads_here = mix_lambda.shape[0]
    query_rows = queries.shape[0]
    value_width = latent_values.shape[1] // heads_here
    empty = (
        jnp.zeros((2, heads_here, query_rows, value_width), jnp.float32),
        jnp.zeros((2, heads_here, query_rows), jnp.float32),
    )
    latent_count = latent_keys.shape[0]
    own_keys = project_heads(context_normed, w_key, key_gain, None, 1.0)
    own_values = jnp.dot(context_normed, w_value, preferred_element_type=jnp.float32).astype(
        jnp.bfloat16
    )
    shard_keys = jnp.concatenate([latent_keys, own_keys], axis=0)
    shard_values = jnp.concatenate([latent_values, own_values], axis=0)
    extra_rows = own_keys.shape[0]
    shard_rows = latent_count + extra_rows
    pieces = sent_together((shard_keys, shard_values), "sp", 0, 1)
    row_index = jnp.arange(pieces[0].shape[0], dtype=jnp.int32) % shard_rows
    lift_rows = jnp.where(row_index[None, :] >= latent_count, context_lift[:, None], 0.0)
    numerator, totals = accumulate_blocks(empty, queries, pieces[0], pieces[1], lift_rows)
    ratios = numerator / totals[..., None]
    mixed_heads = ratios[0] - mix_lambda[:, None, None] * ratios[1]
    inverse = lax.rsqrt(jnp.mean(mixed_heads * mixed_heads, axis=-1, keepdims=True) + head_eps)
    head_out = (mixed_heads * inverse * value_gain * head_factor).astype(jnp.bfloat16)
    out_weight = w_out.reshape(heads_here, value_width, w_out.shape[1])
    mixture = sum_at_owner(
        jnp.einsum("hqe,hed->qd", head_out, out_weight, preferred_element_type=jnp.float32), "tp", 0
    )
    return (latent.astype(jnp.float32) + modulation[4] * mixture).astype(jnp.bfloat16)


def solution(mesh):
    placed = (
        P(("dp", "sp", "tp"), None),
        P(("dp", "sp"), None),
        P(("dp", "sp")),
        P("sp"),
        P(),
        P("sp", "tp"),
        P("sp", "tp"),
        P("sp", "tp"),
        P(None, "tp"),
        P(None, "tp"),
        P(None, "tp"),
        P(),
        P(),
        P("tp"),
        P("tp"),
        P(),
        P("tp", None),
    )
    return jax.shard_map(
        on_device,
        mesh=mesh,
        in_specs=placed,
        out_specs=P(("dp", "sp", "tp"), None),
        check_vma=False,
    )
```

profile of v0, /device:TPU:2, one launch (start us, length us, event | category | flops | bytes accessed | tf_op | source)
XLA Modules:
  0.0 231.5 jit_solution(1074336177027201900)
XLA Ops:
  7.4 1.1 fusion.33
  8.4 1.0 fusion.36
  9.5 1.0 fusion.37
  11.3 15.2 %all-to-all-start = ((f32[16,5,512]{2,1,0:T(8,128)}), f32[16,5,512]{2,1,0:T(8,128)}, u32[]{:S(2)}, u32[]{:S(2)}) async-start(f32[16,5,512]{2,1,0:T(8,128)} %broadcast_in_dim.21), calls=%async_computation | async-start | bytes 524288 | tf_op jit(solution)/shard_map/all_to_all | solution.py:16
  27.1 1.1 fusion.7
  28.7 16.2 %all-to-all-done = f32[16,5,512]{2,1,0:T(8,128)} async-done(((f32[16,5,512]{2,1,0:T(8,128)}), f32[16,5,512]{2,1,0:T(8,128)}, u32[]{:S(2)}, u32[]{:S(2)}) %all-to-all-start) | async-done | bytes 163872 | tf_op jit(solution)/shard_map/all_to_all | solution.py:16
  45.0 1.0 reduce_sum.90
  46.6 4.5 %all-to-all-start.1 = ((f32[4,5,512]{2,1,0:T(8,128)}), f32[4,5,512]{2,1,0:T(8,128)S(1)}, u32[]{:S(2)}, u32[]{:S(2)}) async-start(f32[4,5,512]{2,1,0:T(8,128)} %broadcast_in_dim.22), calls=%async_computation.1 | async-start | bytes 131072 | tf_op jit(solution)/shard_map/all_to_all | solution.py:16
  51.6 1.3 mul.366
  52.9 1.3 mul.331
  55.6 1.1 all-to-all-done.1
  57.3 1.5 fusion.11
  60.5 1.6 fusion.45
  62.7 1.3 multiply_convert_fusion.1
  64.1 1.5 convolution_convert_fusion.1
  65.6 19.4 %all-gather.3.cloned.1.call-done = bf16[256,2048]{1,0:T(8,128)(2,1)} async-done(((bf16[64,2048]{1,0:T(8,128)(2,1)}), bf16[256,2048]{1,0:T(8,128)(2,1)}) %all-gather.3.cloned.1.call-update) | async-done | bytes 1048592 | tf_op jit(solution)/shard_map/all_gather | solution.py:175
  85.0 2.2 bitcast_reduce_fusion.1
  89.4 1.7 copy.89
  94.5 77.1 %all-gather.5.cloned.1.call-done = bf16[4352,512]{1,0:T(8,128)(2,1)} async-done(((bf16[272,512]{1,0:T(8,128)(2,1)}), bf16[4352,512]{1,0:T(8,128)(2,1)}) %all-gather.5.cloned.1.call-update) | async-done | bytes 4456464 | tf_op jit(solution)/shard_map/all_gather | solution.py:36
  171.6 1.0 fusion.41
  172.8 4.5 %fusion.42 = (bf16[4096,256]{1,0:T(8,128)(2,1)}, bf16[4096,256]{1,0:T(8,128)(2,1)}) fusion(bf16[4352,512]{1,0:T(8,128)(2,1)} %all-gather.5.cloned.1.call-done), kind=kLoop, calls=%fused_computation.102 | loop fusion | bytes 8388608 | tf_op jit(solution)/shard_map/slice | solution.py:125
  177.3 21.7 %while.13 = (s32[]{:T(128)}, f32[2,2,256,128]{2,3,0,1:T(8,128)S(1)}, f32[2,2,256]{2,1,0:T(2,128)S(1)}, bf16[8,512,256]{2,1,0:T(8,128)(2,1)}, bf16[8,512,256]{2,1...) while((s32[]{:T(128)}, ...), condition=%wide.region_8.9_spmd.clone, body=%wide.region_6.8_spmd.clone.sunk | while | flops 203686912 | bytes 10125432 | solution.py:135
  177.3 1.1 constant_dynamic-slice_fusion.3
  180.0 1.1 constant_dynamic-slice_fusion.3
  182.8 1.1 constant_dynamic-slice_fusion.3
  185.5 1.1 constant_dynamic-slice_fusion.3
  188.2 1.1 constant_dynamic-slice_fusion.3
  190.9 1.1 constant_dynamic-slice_fusion.3
  193.6 1.1 constant_dynamic-slice_fusion.3
  196.3 1.1 constant_dynamic-slice_fusion.3
  200.6 21.3 %all_to_all.15 = f32[4,64,2048]{2,1,0:T(8,128)S(1)} all-to-all(f32[4,64,2048]{2,1,0:T(8,128)S(1)} %convolution_bitcast_fusion.1), channel_id=1, replica_groups=mesh['sp'=16,'tp'=4,'dp'=8] {'tp'}, dimensions={0} | all-to-all | bytes 4194304 | tf_op jit(solution)/shard_map/all_to_all | solution.py:50
  222.8 1.8 fusion.12
  (153 shorter events, 28.9 us)
Async XLA Ops:
  6.5 193.6 %copy-start = (bf16[256,2048]{1,0:T(8,128)(2,1)S(1)}, bf16[256,2048]{1,0:T(8,128)(2,1)}, u32[]{:S(2)}) copy-start(bf16[256,2048]{1,0:T(8,128)(2,1)} %param.35) | copy-start | bytes 3145732
  6.5 50.8 %copy-start.5 = (bf16[64,2048]{1,0:T(8,128)(2,1)S(1)}, bf16[64,2048]{1,0:T(8,128)(2,1)}, u32[]{:S(2)}) copy-start(bf16[64,2048]{1,0:T(8,128)(2,1)} %param.19) | copy-start | bytes 786436
  6.5 50.8 %copy-start.11 = (f32[2048]{0:T(1024)S(1)}, f32[2048]{0:T(1024)}, u32[]{:S(2)}) copy-start(f32[2048]{0:T(1024)} %param.23) | copy-start | bytes 24580
  6.5 53.8 %copy-start.6 = (bf16[16,2048]{1,0:T(8,128)(2,1)S(1)}, bf16[16,2048]{1,0:T(8,128)(2,1)}, u32[]{:S(2)}) copy-start(bf16[16,2048]{1,0:T(8,128)(2,1)} %param.20) | copy-start | bytes 196612
  6.5 54.0 %copy-start.2 = (bf16[2048,256]{1,0:T(8,128)(2,1)S(1)}, bf16[2048,256]{1,0:T(8,128)(2,1)}, u32[]{:S(2)}) copy-start(bf16[2048,256]{1,0:T(8,128)(2,1)} %param.28) | copy-start | bytes 3145732
  10.5 53.5 %copy-start.3 = (bf16[2048,256]{1,0:T(8,128)(2,1)S(1)}, bf16[2048,256]{1,0:T(8,128)(2,1)}, u32[]{:S(2)}) copy-start(bf16[2048,256]{1,0:T(8,128)(2,1)} %param.29) | copy-start | bytes 3145732
  11.3 33.7 %all-to-all-start = ((f32[16,5,512]{2,1,0:T(8,128)}), f32[16,5,512]{2,1,0:T(8,128)}, u32[]{:S(2)}, u32[]{:S(2)}) async-start(f32[16,5,512]{2,1,0:T(8,128)} %broadcast_in_dim.21), calls=%async_computation | async-start | bytes 524288 | tf_op jit(solution)/shard_map/all_to_all | solution.py:16
  46.6 10.1 %all-to-all-start.1 = ((f32[4,5,512]{2,1,0:T(8,128)}), f32[4,5,512]{2,1,0:T(8,128)S(1)}, u32[]{:S(2)}, u32[]{:S(2)}) async-start(f32[4,5,512]{2,1,0:T(8,128)} %broadcast_in_dim.22), calls=%async_computation.1 | async-start | bytes 131072 | tf_op jit(solution)/shard_map/all_to_all | solution.py:16
  51.0 34.0 %all-gather.3.cloned.1.call-start = ((), (), s32[]{:S(2)}) async-start(), calls=%async_computation.3 | async-start | bytes 1310720 | tf_op jit(solution)/shard_map/all_gather | solution.py:175
  57.3 6.8 %copy-start.12 = (f32[1,4,512]{2,0,1:T(1,128)S(1)}, f32[1,4,512]{2,0,1:T(1,128)}, u32[]{:S(2)}) copy-start(f32[1,4,512]{2,0,1:T(1,128)} %get-tuple-element.141) | copy-start | bytes 24580
  58.8 112.8 %all-gather.5.cloned.1.call-start = ((), (), s32[]{:S(2)}) async-start(), calls=%async_computation.4 | async-start | bytes 4734976 | tf_op jit(solution)/shard_map/all_gather | solution.py:36
  60.5 1.7 copy-start.19
  65.6 22.2 %copy-start.17 = (f32[2,2,16]{2,1,0:T(2,128)S(1)}, f32[2,2,16]{2,1,0:T(2,128)}, u32[]{:S(2)}) copy-start(f32[2,2,16]{2,1,0:T(2,128)} %mul.366) | copy-start | bytes 772
  65.6 22.3 %copy-start.16 = (f32[2,2,16]{2,1,0:T(2,128)S(1)}, f32[2,2,16]{2,1,0:T(2,128)}, u32[]{:S(2)}) copy-start(f32[2,2,16]{2,1,0:T(2,128)} %mul.331) | copy-start | bytes 772
  85.0 2.2 copy-start.1
  87.2 0.8 copy-start.9
  87.2 0.8 copy-start.10
  87.8 3.3 %copy-start.4 = (bf16[2048,256]{1,0:T(8,128)(2,1)S(1)}, bf16[2048,256]{1,0:T(8,128)(2,1)}, u32[]{:S(2)}) copy-start(bf16[2048,256]{1,0:T(8,128)(2,1)} %param.29) | copy-start | bytes 3145732
  87.9 3.7 %copy-start.13 = (bf16[16,256]{1,0:T(8,128)(2,1)S(1)}, bf16[16,256]{1,0:T(8,128)(2,1)}, u32[]{:S(2)}) copy-start(bf16[16,256]{1,0:T(8,128)(2,1)} %convolution_convert_fusion.1) | copy-start | bytes 24580
  87.9 3.7 %copy-start.15 = (bf16[16,256]{1,0:T(8,128)(2,1)S(1)}, bf16[16,256]{1,0:T(8,128)(2,1)}, u32[]{:S(2)}) copy-start(bf16[16,256]{1,0:T(8,128)(2,1)} %multiply_convert_fusion.1) | copy-start | bytes 24580
  91.1 0.9 copy-start.7
  93.6 83.8 %copy-start.8 = (f32[2,4352]{1,0:T(2,128)}, f32[2,4352]{1,0:T(2,128)S(1)}, u32[]{:S(2)}) copy-start(f32[2,4352]{1,0:T(2,128)S(1)} %broadcast_select_fusion) | copy-start | bytes 104452
  177.3 21.7 %slice-start = ((f32[2,4352]{1,0:T(2,128)}), f32[2,256]{1,0:T(2,128)S(1)}, s32[]{:S(2)}) async-start(f32[2,4352]{1,0:T(2,128)} %copy-done.8), calls=%async_computation.5 | async-start | bytes 4096 | tf_op jit(solution)/shard_map/slice | solution.py:137
  199.0 0.7 copy-start.18
  199.0 0.8 copy-start.20
  221.8 1.0 copy-start.14
Sparse Core Ops, SparseCore 0:
  58.9 26.0 all-gather.2
  92.9 78.6 all-gather.4
where the time goes:
time: 232 us; the launch traced here: 231 us
  waiting for transfers between devices  114 us (49%)
  local copies, waits for them, and re-layouts  24.7 us (11%)
  blocking collectives  21.3 us (9%)
  other arithmetic  19.8 us (9%)
  starting transfers between devices  19.8 us (9%)
  matrix products  17.8 us (8%)
  between operations  13.8 us (6%)
    all_gather x1, waiting for transfers between devices, sent_together(): lax.all_gather(both, axis, axis=dim, tiled=True)  77.1 us
    all_to_all x1, blocking collectives, sum_at_owner(): lax.all_to_all(cut_along(array, dim, devices), axis, 0, 0, tiled=True)  21.3 us
    all_to_all x2, starting transfers between devices, copy_for_each(): return lax.all_to_all(copies, axis, split_axis=0, concat_axis=0, tiled=True)  19.7 us
    all_gather x1, waiting for transfers between devices, on_device(): pieces = lax.all_gather(normed, 'tp', axis=0, tiled=True)  19.4 us
    all_to_all x2, waiting for transfers between devices, copy_for_each(): return lax.all_to_all(copies, axis, split_axis=0, concat_axis=0, tiled=True)  17.3 us
    dynamic_slice x24, local copies, waits for them, and re-layouts, accumulate_blocks(): running = lax.scan(scan_step, running, slabs)[0]  10.8 us
    dot_general x9, matrix products, accumulate(): jnp.einsum('qhmd,phmd->mhqp', shaped_query, shaped_keys, preferred_elemen...  4.96 us
  transfers between devices with their start and end apart: 4, of which 4 were waited for; matrix products, arithmetic and copies ran while one was open for 7% of the time, Pallas kernels for 0%

commit v1 on v0

--- a/solution.py
+++ b/solution.py
@@ -9,6 +9,27 @@
 rope_base = 10000.0
 head_factor = 0.8
 key_block = 512
+
+
+def collect_2(x, axis, dim):
+    peers, position, rows = (lax.axis_size(axis), lax.axis_index(axis), x.shape[dim])
+    right = [(i, (i + 1) % peers) for i in range(peers)]
+    backward = [(i, (i - 1) % peers) for i in range(peers)]
+    out = jnp.zeros((*x.shape[:dim], peers * rows, *x.shape[dim + 1 :]), x.dtype)
+    out = lax.dynamic_update_slice_in_dim(out, x, position * rows, axis=dim)
+    from_left = from_right = x
+    half = peers // 2
+    for step in range(1, half + 1):
+        from_left = lax.ppermute(from_left, axis, right)
+        out = lax.dynamic_update_slice_in_dim(
+            out, from_left, (position - step) % peers * rows, axis=dim
+        )
+        if step < peers - half:
+            from_right = lax.ppermute(from_right, axis, backward)
+            out = lax.dynamic_update_slice_in_dim(
+                out, from_right, (position + step) % peers * rows, axis=dim
+            )
+    return out
 
 
 def copy_for_each(array, axis):
@@ -172,7 +193,7 @@
     local_rows = latent.shape[0]
     offset = lax.axis_index("sp") * (local_rows * lax.axis_size("tp"))
     head_width = query_gain.shape[0]
-    pieces = lax.all_gather(normed, "tp", axis=0, tiled=True)
+    pieces = collect_2(normed, "tp", 0)
     positions = offset + jnp.arange(pieces.shape[0], dtype=jnp.int32)
     query_part = project_heads(pieces, w_query, query_gain, positions, head_width ** (-0.5))
     key_part = project_heads(pieces, w_key, key_gain, positions, 1.0)

time: 232 us -> 268 us (1.16)
  matrix products: 17.8 us -> 44.2 us
  local copies, waits for them, and re-layouts: 24.7 us -> 46 us
  waiting for transfers between devices: 114 us -> 95.1 us
  starting transfers between devices: 19.8 us -> 28.6 us
  other arithmetic: 19.8 us -> 16.4 us
    all_gather x1 -> x0, waiting for transfers between devices: 19.4 us -> none  [on_device(): pieces = lax.all_gather(normed, 'tp', axis=0, tiled=True)]
    dot_general x9, matrix products: 3.01 us -> 21.6 us  [accumulate(): jnp.einsum('mhqp,phe->mhqe', weights.astype(jnp.bfloat16), shaped_values,...]
    dynamic_slice x24, local copies, waits for them, and re-layouts: 10.8 us -> 24 us  [accumulate_blocks(): running = lax.scan(scan_step, running, slabs)[0]]
    ppermute x0 -> x3, starting transfers between devices: none -> 8.96 us  [the longest x1 4.58 us: collect_2(): from_right = lax.ppermute(from_right, axis, backward)]
    dot_general x9, matrix products: 4.96 us -> 13.7 us  [accumulate(): jnp.einsum('qhmd,phmd->mhqp', shaped_query, shaped_keys, preferred_elemen...]
    all_gather x1, waiting for transfers between devices: 77.1 us -> 70 us  [sent_together(): lax.all_gather(both, axis, axis=dim, tiled=True)]
    ppermute x0 -> x3, waiting for transfers between devices: none -> 6.53 us  [the longest x2 6.53 us: collect_2(): from_left = lax.ppermute(from_left, axis, right)]
    add x8, local copies, waits for them, and re-layouts: 0.05 us -> 5.47 us  [accumulate(): weights = jnp.exp(scores + lift_rows[None, :, None, :])]
  transfers between devices with their start and end apart: 4 -> 6, of which waited for: 4 -> 4; matrix products, arithmetic and copies ran while one was open for 7% -> 6% of each run, Pallas kernels for 0% -> 0%
where the time goes in v1:
time: 268 us; the launch traced here: 266 us
  waiting for transfers between devices  95.1 us (35%)
  local copies, waits for them, and re-layouts  46 us (17%)
  matrix products  44.2 us (16%)
  starting transfers between devices  28.6 us (11%)
  blocking collectives  21.2 us (8%)
  other arithmetic  16.4 us (6%)
  between operations  13.9 us (5%)
    all_gather x1, waiting for transfers between devices, sent_together(): lax.all_gather(both, axis, axis=dim, tiled=True)  70 us
    dynamic_slice x24, local copies, waits for them, and re-layouts, accumulate_blocks(): running = lax.scan(scan_step, running, slabs)[0]  24 us
    dot_general x9, matrix products, accumulate(): jnp.einsum('mhqp,phe->mhqe', weights.astype(jnp.bfloat16), shaped_values,...  21.6 us
    all_to_all x1, blocking collectives, sum_at_owner(): lax.all_to_all(cut_along(array, dim, devices), axis, 0, 0, tiled=True)  21.2 us
    all_to_all x2, starting transfers between devices, copy_for_each(): return lax.all_to_all(copies, axis, split_axis=0, concat_axis=0, tiled=True)  19.7 us
    all_to_all x2, waiting for transfers between devices, copy_for_each(): return lax.all_to_all(copies, axis, split_axis=0, concat_axis=0, tiled=True)  18.5 us
    dot_general x9, matrix products, accumulate(): jnp.einsum('qhmd,phmd->mhqp', shaped_query, shaped_keys, preferred_elemen...  13.7 us
    ppermute x2, waiting for transfers between devices, collect_2(): from_left = lax.ppermute(from_left, axis, right)  6.53 us
  transfers between devices with their start and end apart: 6, of which 4 were waited for; matrix products, arithmetic and copies ran while one was open for 6% of the time, Pallas kernels for 0%

profile of v1, /device:TPU:2, one launch (start us, length us, event | category | flops | bytes accessed | tf_op | source)
XLA Modules:
  0.0 265.8 jit_solution(3963134892507198432)
XLA Ops:
  11.3 15.2 %all-to-all-start = ((f32[16,5,512]{2,1,0:T(8,128)}), f32[16,5,512]{2,1,0:T(8,128)S(1)}, u32[]{:S(2)}, u32[]{:S(2)}) async-start(f32[16,5,512]{2,1,0:T(8,128)} %broadcast_in_dim.23), calls=%async_computation | async-start | bytes 524288 | tf_op jit(solution)/shard_map/all_to_all | solution.py:37
  29.8 15.1 %all-to-all-done = f32[16,5,512]{2,1,0:T(8,128)S(1)} async-done(((f32[16,5,512]{2,1,0:T(8,128)}), f32[16,5,512]{2,1,0:T(8,128)S(1)}, u32[]{:S(2)}, u32[]{:S(2)}) %all-to-all-start) | async-done | bytes 163872 | tf_op jit(solution)/shard_map/all_to_all | solution.py:37
  45.6 4.5 %all-to-all-start.1 = ((f32[4,5,512]{2,1,0:T(8,128)}), f32[4,5,512]{2,1,0:T(8,128)S(1)}, u32[]{:S(2)}, u32[]{:S(2)}) async-start(f32[4,5,512]{2,1,0:T(8,128)} %broadcast_in_dim.24), calls=%async_computation.1 | async-start | bytes 131072 | tf_op jit(solution)/shard_map/all_to_all | solution.py:37
  52.2 3.4 %all-to-all-done.1 = f32[4,5,512]{2,1,0:T(8,128)S(1)} async-done(((f32[4,5,512]{2,1,0:T(8,128)}), f32[4,5,512]{2,1,0:T(8,128)S(1)}, u32[]{:S(2)}, u32[]{:S(2)}) %all-to-all-start.1) | async-done | bytes 40992 | tf_op jit(solution)/shard_map/all_to_all | solution.py:37
  57.9 2.5 collective-permute-start
  60.4 4.6 %collective-permute-start.1 = (bf16[64,2048]{1,0:T(8,128)(2,1)}, bf16[64,2048]{1,0:T(8,128)(2,1)}, u32[]{:S(2)}, u32[]{:S(2)}) collective-permute-start(bf16[64,2048]{1,0:T(8,128)(2,1)} %get-tuple-element.126), channel_id=1, source_target_pairs={{0,24},{8,0},{16,8},{24,16},{1,25},{9,1},{17,9},{25,17},{2,26},{10... | collective-permute-start | bytes 786440 | tf_op jit(solution)/shard_map/ppermute | solution.py:28
  70.8 2.1 convolution_convert_fusion.1
  74.7 1.9 collective-permute-start.2
  77.7 6.5 %collective-permute-done.2 = bf16[64,2048]{1,0:T(8,128)(2,1)S(1)} collective-permute-done((bf16[64,2048]{1,0:T(8,128)(2,1)S(1)}, bf16[64,2048]{1,0:T(8,128)(2,1)S(1)}, u32[]{:S(2)}, u32[]{:S(2)}) %collective-permute-start.2) | collective-permute-done | bytes 262176 | tf_op jit(solution)/shard_map/ppermute | solution.py:23
  88.0 70.0 %all-gather.2.cloned.1.call-done = bf16[4352,512]{1,0:T(8,128)(2,1)} async-done(((bf16[272,512]{1,0:T(8,128)(2,1)}), bf16[4352,512]{1,0:T(8,128)(2,1)}) %all-gather.2.cloned.1.call-update) | async-done | bytes 4456464 | tf_op jit(solution)/shard_map/all_gather | solution.py:57
  158.0 1.6 fusion.42
  160.4 4.5 %fusion.43 = (bf16[4096,256]{1,0:T(8,128)(2,1)}, bf16[4096,256]{1,0:T(8,128)(2,1)}) fusion(bf16[4352,512]{1,0:T(8,128)(2,1)} %all-gather.2.cloned.1.call-done), kind=kLoop, calls=%fused_computation.106 | loop fusion | bytes 8388608 | tf_op jit(solution)/shard_map/slice | solution.py:146
  165.0 65.5 %while.13 = (s32[]{:T(128)}, f32[2,2,256,128]{2,3,0,1:T(8,128)}, f32[2,2,256]{2,1,0:T(2,128)S(1)}, bf16[8,512,256]{2,1,0:T(8,128)(2,1)}, bf16[8,512,256]{2,1,0:T...) while((s32[]{:T(128)}, f32[2,2,256,128]{2,3,0,1:T(8,128)}, ...), condition=%wide.region_8.9_spmd.clone, body=%wide.region_6.8_spmd.clone.sunk | while | flops 203686912 | bytes 10125424 | solution.py:156
  165.0 1.8 constant_dynamic-slice_fusion.3
  170.2 2.4 fusion.71
  173.0 1.8 constant_dynamic-slice_fusion.3
  178.3 2.6 fusion.71
  181.2 1.8 constant_dynamic-slice_fusion.3
  186.5 2.6 fusion.71
  189.4 1.8 constant_dynamic-slice_fusion.3
  194.7 2.6 fusion.71
  197.6 1.8 constant_dynamic-slice_fusion.3
  200.2 1.6 bitcast_convert_fusion.2
  202.9 2.6 fusion.71
  205.8 1.8 constant_dynamic-slice_fusion.3
  211.1 2.6 fusion.71
  214.0 1.8 constant_dynamic-slice_fusion.3
  219.3 2.6 fusion.71
  222.2 1.8 constant_dynamic-slice_fusion.3
  227.5 2.6 fusion.71
  235.0 21.2 %all_to_all.15 = f32[4,64,2048]{2,1,0:T(8,128)S(1)} all-to-all(f32[4,64,2048]{2,1,0:T(8,128)S(1)} %convolution_bitcast_fusion.1), channel_id=1, replica_groups=mesh['sp'=16,'tp'=4,'dp'=8] {'tp'}, dimensions={0} | all-to-all | bytes 4194304 | tf_op jit(solution)/shard_map/all_to_all | solution.py:71
  257.2 1.8 fusion.12
  (153 shorter events, 60.5 us)
Async XLA Ops:
  6.5 228.0 %copy-start = (bf16[256,2048]{1,0:T(8,128)(2,1)S(1)}, bf16[256,2048]{1,0:T(8,128)(2,1)}, u32[]{:S(2)}) copy-start(bf16[256,2048]{1,0:T(8,128)(2,1)} %param.35) | copy-start | bytes 3145732
  6.5 49.9 %copy-start.3 = (bf16[64,2048]{1,0:T(8,128)(2,1)S(1)}, bf16[64,2048]{1,0:T(8,128)(2,1)}, u32[]{:S(2)}) copy-start(bf16[64,2048]{1,0:T(8,128)(2,1)} %param.19) | copy-start | bytes 786436
  6.5 43.7 %copy-start.14 = (f32[64]{0:T(128)S(1)}, f32[64]{0:T(128)}, u32[]{:S(2)}) copy-start(f32[64]{0:T(128)} %param.31) | copy-start | bytes 772
  6.5 44.4 %copy-start.17 = (f32[64]{0:T(128)S(1)}, f32[64]{0:T(128)}, u32[]{:S(2)}) copy-start(f32[64]{0:T(128)} %param.30) | copy-start | bytes 772
  6.5 49.9 %copy-start.7 = (f32[2048]{0:T(1024)S(1)}, f32[2048]{0:T(1024)}, u32[]{:S(2)}) copy-start(f32[2048]{0:T(1024)} %param.23) | copy-start | bytes 24580
  8.4 56.6 %copy-start.1 = (bf16[2048,256]{1,0:T(8,128)(2,1)S(1)}, bf16[2048,256]{1,0:T(8,128)(2,1)}, u32[]{:S(2)}) copy-start(bf16[2048,256]{1,0:T(8,128)(2,1)} %param.28) | copy-start | bytes 3145732
  8.4 56.6 %copy-start.6 = (bf16[16,2048]{1,0:T(8,128)(2,1)S(1)}, bf16[16,2048]{1,0:T(8,128)(2,1)}, u32[]{:S(2)}) copy-start(bf16[16,2048]{1,0:T(8,128)(2,1)} %param.20) | copy-start | bytes 196612
  11.3 33.6 %all-to-all-start = ((f32[16,5,512]{2,1,0:T(8,128)}), f32[16,5,512]{2,1,0:T(8,128)S(1)}, u32[]{:S(2)}, u32[]{:S(2)}) async-start(f32[16,5,512]{2,1,0:T(8,128)} %broadcast_in_dim.23), calls=%async_computation | async-start | bytes 524288 | tf_op jit(solution)/shard_map/all_to_all | solution.py:37
  45.6 10.1 %all-to-all-start.1 = ((f32[4,5,512]{2,1,0:T(8,128)}), f32[4,5,512]{2,1,0:T(8,128)S(1)}, u32[]{:S(2)}, u32[]{:S(2)}) async-start(f32[4,5,512]{2,1,0:T(8,128)} %broadcast_in_dim.24), calls=%async_computation.1 | async-start | bytes 131072 | tf_op jit(solution)/shard_map/all_to_all | solution.py:37
  50.0 108.0 %all-gather.2.cloned.1.call-start = ((), (), s32[]{:S(2)}) async-start(), calls=%async_computation.3 | async-start | bytes 4734976 | tf_op jit(solution)/shard_map/all_gather | solution.py:57
  56.3 8.7 %copy-start.8 = (f32[1,4,512]{2,0,1:T(1,128)}, f32[1,4,512]{2,0,1:T(1,128)S(1)}, u32[]{:S(2)}) copy-start(f32[1,4,512]{2,0,1:T(1,128)S(1)} %get-tuple-element.143) | copy-start | bytes 24580
  57.9 16.8 %collective-permute-start = (bf16[64,2048]{1,0:T(8,128)(2,1)}, bf16[64,2048]{1,0:T(8,128)(2,1)S(1)}, u32[]{:S(2)}, u32[]{:S(2)}) collective-permute-start(bf16[64,2048]{1,0:T(8,128)(2,1)} %get-tuple-element.126), channel_id=1, source_target_pairs={{0,8},{8,16},{16,24},{24,0},{1,9},{9,17},{17,25},{25,1},{2,10},{10... | collective-permute-start | bytes 786440 | tf_op jit(solution)/shard_map/ppermute | solution.py:23
  60.4 16.3 %collective-permute-start.1 = (bf16[64,2048]{1,0:T(8,128)(2,1)}, bf16[64,2048]{1,0:T(8,128)(2,1)}, u32[]{:S(2)}, u32[]{:S(2)}) collective-permute-start(bf16[64,2048]{1,0:T(8,128)(2,1)} %get-tuple-element.126), channel_id=1, source_target_pairs={{0,24},{8,0},{16,8},{24,16},{1,25},{9,1},{17,9},{25,17},{2,26},{10... | collective-permute-start | bytes 786440 | tf_op jit(solution)/shard_map/ppermute | solution.py:28
  73.9 10.9 %copy-start.2 = (bf16[2048,256]{1,0:T(8,128)(2,1)S(1)}, bf16[2048,256]{1,0:T(8,128)(2,1)}, u32[]{:S(2)}) copy-start(bf16[2048,256]{1,0:T(8,128)(2,1)} %param.29) | copy-start | bytes 3145732
  74.7 9.5 %collective-permute-start.2 = (bf16[64,2048]{1,0:T(8,128)(2,1)S(1)}, bf16[64,2048]{1,0:T(8,128)(2,1)S(1)}, u32[]{:S(2)}, u32[]{:S(2)}) collective-permute-start(bf16[64,2048]{1,0:T(8,128)(2,1)S(1)} %collective-permute-done), channel_id=1, source_target_pairs={{0,8},{8,16},{16,24},{24,0},{1,9},{9,17},{17,25},{25,1},{2,10},{10... | collective-permute-start | bytes 786440 | tf_op jit(solution)/shard_map/ppermute | solution.py:23
  84.2 1.2 copy-start.5
  84.8 1.3 copy-start.12
  84.8 1.3 copy-start.11
  85.5 1.0 copy-start.9
  86.0 1.2 copy-start.15
  230.5 3.7 %copy-start.13 = (f32[2]{0:T(128)S(1)}, f32[2]{0:T(128)}, u32[]{:S(2)}) copy-start(f32[2]{0:T(128)} %param.32) | copy-start | bytes 28
  230.5 3.8 %copy-start.16 = (f32[128]{0:T(128)S(1)}, f32[128]{0:T(128)}, u32[]{:S(2)}) copy-start(f32[128]{0:T(128)} %param.34) | copy-start | bytes 1540
  256.2 1.0 copy-start.4
  256.2 1.0 copy-start.10
Sparse Core Ops, SparseCore 0:
  87.3 70.6 all-gather.1
